TPU v7x, 32 devices: a whole 2x2x4 slice. The times are simulated.
32 devices in a mesh: ep: 16 (over z, y, core), tp: 2 (over x).
Axes of the slice: x: 2, y: 2, z: 4, core: 2. Of those that a mesh axis runs over, the one named last changes fastest.
Arguments:
- tokens: bfloat16 [128, 1024], P(('ep', 'tp')), may hold values from -6 to 6
- lengths: int32 [128], P(('ep', 'tp')), may hold values from 256 to 1024, as said below
- cache_latent: bfloat16 [128, 1024, 256], P(('ep', 'tp')), may hold values from -160 to 160
- cache_rope: bfloat16 [128, 32, 1024], P(('ep', 'tp')), may hold values from -6 to 6
- attn_gain: float32 [1024], replicated, may hold values from 0.1 to 1.9
- latent_gain: float32 [256], replicated, may hold values from 0.1 to 1.9
- post_gain: float32 [1024], replicated, may hold values from 0.1 to 1.9
- ffn_gain: float32 [1024], replicated, may hold values from 0.1 to 1.9
- out_gain: float32 [1024], replicated, may hold values from 0.1 to 1.9
- w_latent: bfloat16 [1024, 256], P(None, 'tp'), may hold values from -0.1875 to 0.1875
- w_rope_key: bfloat16 [1024, 32], replicated, may hold values from -0.1875 to 0.1875
- w_query: bfloat16 [1024, 768], P(None, 'tp'), may hold values from -0.1875 to 0.1875
- w_absorb_key: bfloat16 [8, 64, 256], P('tp'), may hold values from -0.75 to 0.75
- w_absorb_value: bfloat16 [8, 256, 64], P('tp'), may hold values from -0.375 to 0.375
- w_out: bfloat16 [512, 1024], P('tp'), may hold values from -0.25 to 0.25
- routes: int32 [128, 6], P(('ep', 'tp')), may hold values from 0 to 15, all different within a row; in each aligned block of 8 rows (0 to 7, 8 to 15, ...) at most 5 rows name the same one
- route_weights: float32 [128, 6], P(('ep', 'tp')), may hold values from 0.2 to 1
- w_exp_gate: bfloat16 [16, 1024, 256], P('ep'), may hold values from -0.1875 to 0.1875
- w_exp_up: bfloat16 [16, 1024, 256], P('ep'), may hold values from -0.1875 to 0.1875
- w_exp_down: bfloat16 [16, 256, 1024], P('ep'), may hold values from -0.375 to 0.375
- w_dense_gate: bfloat16 [4096, 1024], P('ep'), may hold values from -0.1875 to 0.1875
- w_dense_up: bfloat16 [4096, 1024], P('ep'), may hold values from -0.1875 to 0.1875
- w_dense_down: bfloat16 [4096, 1024], P('ep'), may hold values from -0.09375 to 0.09375
- dense_gate_vector: float32 [1024], replicated, may hold values from -0.1875 to 0.1875
Outputs:
- output: bfloat16 [128, 1024], P(('ep', 'tp'))
- new_latent: bfloat16 [128, 256], P(('ep', 'tp'))
- new_rope_key: bfloat16 [128, 32], P(('ep', 'tp'))
Inputs may be any that keep to these rules, and one draw needn't show every extreme that they name: `routes`: in each aligned block of 8 rows no expert is named by more than 5 rows; each row names 6 different experts. `lengths`: some sequence holds exactly 1024 cached positions.
All inputs are finite; a program needn't handle non-finite values.
Results may differ from a plain program's by a relative error of at most 0.015.
Values may be sent and summed in bfloat16 or wider, within the bound.
No kernel may reach another device: no remote copies, remote signals or barrier semaphores. Data moves between devices by JAX's collectives and lax.ppermute only.
A program may use at most 64 MiB of HBM per device.

v0:
```python
import jax
import jax.numpy as jnp
from jax import lax
from jax.sharding import PartitionSpec as P

epsilon = 1e-06
rope_base = 10000.0
negative = -1e30


def normalize(values, gain_vec):
    values = values.astype(jnp.float32)
    return (
        values * lax.rsqrt(jnp.mean(values * values, axis=-1, keepdims=True) + epsilon) * gain_vec
    )


def rotate(values, positions):
    half_width = values.shape[-1] // 2
    inverse = rope_base ** (-jnp.arange(half_width, dtype=jnp.float32) / half_width)
    angles = positions.astype(jnp.float32)[..., None] * inverse
    cosine = jnp.cos(angles)
    sine_part = jnp.sin(angles)
    first_half = values[..., :half_width]
    second = values[..., half_width:]
    return jnp.concatenate(
        [first_half * cosine - second * sine_part, first_half * sine_part + second * cosine],
        axis=-1,
    )


def attend(q_latent, q_rope, cache_lat, cache_rot, new_lat, new_rot, seq_lengths, scaling):
    scores = jnp.einsum("shc,slc->shl", q_latent, cache_lat, preferred_element_type=jnp.float32)
    scores = scores + jnp.einsum(
        "shr,srl->shl", q_rope, cache_rot, preferred_element_type=jnp.float32
    )
    scores = scores * scaling
    own_score = jnp.sum(
        q_latent.astype(jnp.float32) * new_lat.astype(jnp.float32)[:, None, :], axis=-1
    )
    own_score = (
        own_score
        + jnp.sum(q_rope.astype(jnp.float32) * new_rot.astype(jnp.float32)[:, None, :], axis=-1)
    ) * scaling
    visible = (
        jnp.arange(cache_lat.shape[1], dtype=jnp.int32)[None, None, :] < seq_lengths[:, None, None]
    )
    scores = jnp.where(visible, scores, negative)
    row_max = jnp.maximum(jnp.max(scores, axis=-1), own_score)
    weights = jnp.exp(scores - row_max[..., None])
    own_weight = jnp.exp(own_score - row_max)
    totals = jnp.sum(weights, axis=-1) + own_weight
    probabilities = (weights / totals[..., None]).astype(jnp.bfloat16)
    own_prob = (own_weight / totals).astype(jnp.bfloat16)
    mixed = jnp.einsum("shl,slc->shc", probabilities, cache_lat, preferred_element_type=jnp.float32)
    mixed = (
        mixed + own_prob.astype(jnp.float32)[..., None] * new_lat.astype(jnp.float32)[:, None, :]
    )
    return mixed.astype(jnp.bfloat16)


def expert_rows(rows_in, gate_w, up_w, down_w):
    model_width = rows_in.shape[-1]
    flattened = rows_in.reshape(-1, model_width)
    gate_pre = jnp.dot(flattened, gate_w, preferred_element_type=jnp.float32)
    up_proj = jnp.dot(flattened, up_w, preferred_element_type=jnp.float32)
    activity = (jax.nn.silu(gate_pre) * up_proj).astype(jnp.bfloat16)
    result = jnp.dot(activity, down_w, preferred_element_type=jnp.float32).astype(jnp.bfloat16)
    return result.reshape(rows_in.shape)


def rank_in_expert(flattened, experts):
    route_count = flattened.shape[0]
    onehot = (flattened[:, None] == jnp.arange(experts, dtype=jnp.int32)[None, :]).astype(
        jnp.float32
    )
    strictly = (jnp.arange(route_count)[:, None] > jnp.arange(route_count)[None, :]).astype(
        jnp.float32
    )
    earlier = jnp.dot(strictly, onehot, precision=lax.Precision.HIGHEST)
    return jnp.sum(earlier * onehot, axis=1).astype(jnp.int32)


def shards(
    tokens,
    lengths,
    cache_latent,
    cache_rope,
    attn_gain,
    latent_gain,
    post_gain,
    ffn_gain,
    out_gain,
    w_latent,
    w_rope_key,
    w_query,
    w_absorb_key,
    w_absorb_value,
    w_out,
    routes,
    route_weights,
    w_exp_gate,
    w_exp_up,
    w_exp_down,
    w_dense_gate,
    w_dense_up,
    w_dense_down,
    dense_gate_vector,
):
    own_rows = tokens.shape[0]
    model_width = tokens.shape[1]
    tp_count = lax.axis_size("tp")
    ep_count = lax.axis_size("ep")
    rope_width = w_rope_key.shape[1]
    nope_width = w_absorb_key.shape[1]
    head_span = nope_width + rope_width
    scaling = head_span ** (-0.5)
    top_count = routes.shape[1]
    group_size = own_rows * tp_count
    capacity = min(
        group_size, max(2, (3 * group_size * top_count + 2 * ep_count - 1) // (2 * ep_count))
    )
    hidden = normalize(tokens, attn_gain).astype(jnp.bfloat16)
    new_rope_key = rotate(
        jnp.dot(hidden, w_rope_key, preferred_element_type=jnp.float32), lengths
    ).astype(jnp.bfloat16)
    local_heads = w_absorb_key.shape[0]
    group_hidden = lax.all_gather(hidden, "tp", axis=0, tiled=True)
    latent_part = jnp.dot(group_hidden, w_latent, preferred_element_type=jnp.float32)
    latent_full = lax.all_to_all(latent_part, "tp", split_axis=0, concat_axis=1, tiled=True)
    new_latent = normalize(latent_full, latent_gain).astype(jnp.bfloat16)
    queries = jnp.dot(group_hidden, w_query, preferred_element_type=jnp.float32).astype(
        jnp.bfloat16
    )
    queries = queries.reshape(group_size, local_heads, head_span)
    query_latent = jnp.einsum(
        "shn,hnc->shc", queries[..., :nope_width], w_absorb_key, preferred_element_type=jnp.float32
    ).astype(jnp.bfloat16)
    query_latent, query_rope = (
        lax.all_to_all(query_latent, "tp", split_axis=0, concat_axis=1, tiled=True),
        lax.all_to_all(queries[..., nope_width:], "tp", split_axis=0, concat_axis=1, tiled=True),
    )
    query_rope = rotate(query_rope.astype(jnp.float32), lengths[:, None]).astype(jnp.bfloat16)
    attended = attend(
        query_latent,
        query_rope,
        cache_latent,
        cache_rope,
        new_latent,
        new_rope_key,
        lengths,
        scaling,
    )
    attended = lax.all_to_all(attended, "tp", split_axis=1, concat_axis=0, tiled=True)
    head_out = (
        jnp.einsum("shc,hcv->shv", attended, w_absorb_value, preferred_element_type=jnp.float32)
        .astype(jnp.bfloat16)
        .reshape(group_size, -1)
    )
    mixed = lax.psum_scatter(
        jnp.dot(head_out, w_out, preferred_element_type=jnp.float32).astype(jnp.bfloat16),
        "tp",
        scatter_dimension=0,
        tiled=True,
    ).astype(jnp.float32)
    residual = (tokens.astype(jnp.float32) + normalize(mixed, post_gain)).astype(jnp.bfloat16)
    ffn_in = normalize(residual, ffn_gain).astype(jnp.bfloat16)
    gate_w = w_exp_gate[0]
    up_w = w_exp_up[0]
    down_w = w_exp_down[0]
    flattened = routes.reshape(-1)
    order_rank = rank_in_expert(flattened, ep_count)
    slot_index = (flattened * capacity + order_rank).reshape(own_rows, top_count)
    dispatch = jnp.any(
        slot_index[None, :, :] == jnp.arange(ep_count * capacity, dtype=jnp.int32)[:, None, None],
        axis=-1,
    ).astype(jnp.bfloat16)
    outgoing = jnp.dot(dispatch, ffn_in, preferred_element_type=jnp.float32).astype(jnp.bfloat16)
    outgoing = outgoing.reshape(ep_count, capacity, model_width)
    result = expert_rows(
        lax.all_to_all(outgoing, "ep", split_axis=0, concat_axis=0, tiled=True),
        gate_w,
        up_w,
        down_w,
    )
    returned = lax.all_to_all(result, "ep", split_axis=0, concat_axis=0, tiled=True)
    picked = returned.reshape(ep_count * capacity, model_width)[slot_index].astype(jnp.float32)
    routed = jnp.sum(route_weights[..., None] * picked, axis=1)
    piece_rows = lax.all_gather(ffn_in, "ep", axis=0, tiled=True)
    dims = (((1,), (1,)), ((), ()))
    gate_pre = lax.dot_general(piece_rows, w_dense_gate, dims, preferred_element_type=jnp.float32)
    up_proj = lax.dot_general(piece_rows, w_dense_up, dims, preferred_element_type=jnp.float32)
    dense_act = (jax.nn.silu(gate_pre) * up_proj).astype(jnp.bfloat16)
    dense_out = lax.psum_scatter(
        jnp.dot(dense_act, w_dense_down, preferred_element_type=jnp.float32),
        "ep",
        scatter_dimension=0,
        tiled=True,
    )
    dense_gate = jax.nn.sigmoid(jnp.sum(ffn_in.astype(jnp.float32) * dense_gate_vector, axis=-1))
    combined = routed + dense_gate[:, None] * dense_out
    output = (residual.astype(jnp.float32) + normalize(combined, out_gain)).astype(jnp.bfloat16)
    return (output, new_latent, new_rope_key)


def solution(mesh):
    placed = (
        P(("ep", "tp"), None),
        P(("ep", "tp")),
        P(("ep", "tp"), None, None),
        P(("ep", "tp"), None, None),
        P(),
        P(),
        P(),
        P(),
        P(),
        P(None, "tp"),
        P(),
        P(None, "tp"),
        P("tp", None, None),
        P("tp", None, None),
        P("tp", None),
        P(("ep", "tp"), None),
        P(("ep", "tp"), None),
        P("ep", None, None),
        P("ep", None, None),
        P("ep", None, None),
        P("ep", None),
        P("ep", None),
        P("ep", None),
        P(),
    )
    return jax.shard_map(
        shards,
        mesh=mesh,
        in_specs=placed,
        out_specs=(P(("ep", "tp"), None), P(("ep", "tp"), None), P(("ep", "tp"), None)),
        check_vma=False,
    )
```

profile of v0, /device:TPU:0, one launch (start us, length us, event | category | flops | bytes accessed | tf_op | source)
XLA Modules:
  0.0 204.9 jit_solution(364668685929764041)
XLA Ops:
  7.2 1.0 fusion.31
  8.2 0.8 fusion.54
  9.0 5.3 %all-gather = bf16[2,4,1024]{2,1,0:T(4,128)(2,1)S(1)} all-gather(bf16[1,4,1024]{2,1,0:T(4,128)(2,1)S(1)} %fusion.54), channel_id=1, replica_groups=mesh['ep'=16,'tp'=2] {'tp'}, dimensions={0}, use_global_device_ids=true | all-gather | bytes 24576 | tf_op jit(solution)/shard_map/all_gather | solution.py:128
  14.2 1.3 convolution_convert_fusion.5
  15.8 0.7 reshape.295
  16.4 3.3 %all-to-all-start.1 = ((bf16[2,2,256]{2,1,0:T(2,128)(2,1)}), bf16[2,2,256]{2,1,0:T(2,128)(2,1)S(1)}, u32[]{:S(2)}, u32[]{:S(2)}) async-start(bf16[2,2,256]{2,1,0:T(2,128)(2,1)} %reshape.295), calls=%async_computation.1 | async-start | bytes 4096 | tf_op jit(solution)/shard_map/all_to_all | solution.py:141
  19.8 0.7 convert_element_type.152
  20.4 0.7 iota_compare_fusion
  21.1 1.1 fusion.52
  22.2 1.7 fusion.62
  23.9 0.8 eq.28
  24.9 0.7 compare_select_fusion
  25.6 1.0 fusion.6
  26.7 0.6 fusion.57
  27.4 0.6 copy.49
  28.1 3.3 %all-to-all-start.2 = ((f32[2,4,128]{2,1,0:T(4,128)}), f32[2,4,128]{2,1,0:T(4,128)S(1)}, u32[]{:S(2)}, u32[]{:S(2)}) async-start(f32[2,4,128]{2,1,0:T(4,128)} %bitcast.9), calls=%async_computation.2 | async-start | bytes 8192 | tf_op jit(solution)/shard_map/all_to_all | solution.py:130
  31.7 3.5 %all-to-all-done.2 = f32[2,4,128]{2,1,0:T(4,128)S(1)} async-done(((f32[2,4,128]{2,1,0:T(4,128)}), f32[2,4,128]{2,1,0:T(4,128)S(1)}, u32[]{:S(2)}, u32[]{:S(2)}) %all-to-all-start.2) | async-done | bytes 4128 | tf_op jit(solution)/shard_map/all_to_all | solution.py:130
  35.2 3.2 %all-to-all-start = ((bf16[8,4,256]{2,1,0:T(4,128)(2,1)}), bf16[8,4,256]{2,1,0:T(4,128)(2,1)S(1)}, u32[]{:S(2)}, u32[]{:S(2)}) async-start(bf16[8,4,256]{2,1,0:T(4,128)(2,1)} %copy.49), calls=%async_computation | async-start | bytes 32768 | tf_op jit(solution)/shard_map/all_to_all | solution.py:140
  38.5 1.3 fusion.58
  39.9 2.4 %all-to-all-done = bf16[8,4,256]{2,1,0:T(4,128)(2,1)S(1)} async-done(((bf16[8,4,256]{2,1,0:T(4,128)(2,1)}), bf16[8,4,256]{2,1,0:T(4,128)(2,1)S(1)}, u32[]{:S(2)}, u32[]{:S(2)}) %all-to-all-start) | async-done | bytes 16416 | tf_op jit(solution)/shard_map/all_to_all | solution.py:140
  42.6 0.6 fusion.61
  43.3 0.3 fusion.60
  43.6 0.2 fusion.14
  43.8 0.4 fusion.5
  44.2 0.6 copy.55
  44.8 3.2 %all-to-all-start.3 = ((bf16[4,8,256]{2,0,1:T(4,128)(2,1)}), bf16[4,8,256]{2,0,1:T(4,128)(2,1)S(1)}, u32[]{:S(2)}, u32[]{:S(2)}) async-start(bf16[4,8,256]{2,0,1:T(4,128)(2,1)} %copy.55), calls=%async_computation.3 | async-start | bytes 32768 | tf_op jit(solution)/shard_map/all_to_all | solution.py:154
  48.3 0.6 dynamic-slice
  49.5 2.4 %all-to-all-done.3 = bf16[4,8,256]{2,0,1:T(4,128)(2,1)S(1)} async-done(((bf16[4,8,256]{2,0,1:T(4,128)(2,1)}), bf16[4,8,256]{2,0,1:T(4,128)(2,1)S(1)}, u32[]{:S(2)}, u32[]{:S(2)}) %all-to-all-start.3) | async-done | bytes 16416 | tf_op jit(solution)/shard_map/all_to_all | solution.py:154
  52.2 0.2 convolution_convert_fusion.3
  52.4 6.7 %all-reduce = bf16[8,1024]{1,0:T(8,128)(2,1)S(1)} all-reduce(bf16[8,1024]{1,0:T(8,128)(2,1)S(1)} %convolution_convert_fusion.3), channel_id=2, replica_groups=mesh['ep'=16,'tp'=2] {'tp'}, use_global_device_ids=true, to_apply=%region_6.7.clone | all-reduce | flops 8192 | bytes 32768
  59.3 0.2 fusion.35
  59.5 0.7 multiply_reduce_fusion.3
  60.2 0.2 convolution_convert_fusion.1
  60.5 0.8 reshape.272
  61.2 6.4 %all-to-all-start.4 = ((bf16[16,5,1024]{2,1,0:T(8,128)(2,1)}), bf16[16,5,1024]{2,1,0:T(8,128)(2,1)S(1)}, u32[]{:S(2)}, u32[]{:S(2)}) async-start(bf16[16,5,1024]{2,1,0:T(8,128)(2,1)} %reshape.272), calls=%async_computation.4 | async-start | bytes 524288 | tf_op jit(solution)/shard_map/all_to_all | solution.py:181
  67.6 1.3 dynamic-slice.2
  69.6 22.1 %all-gather.1 = bf16[16,4,1024]{2,1,0:T(4,128)(2,1)S(1)} all-gather(bf16[1,4,1024]{2,1,0:T(4,128)(2,1)S(1)} %bitcast.76), channel_id=1, replica_groups=mesh['ep'=16,'tp'=2] {'ep'}, dimensions={0}, use_global_device_ids=true | all-gather | bytes 139264 | tf_op jit(solution)/shard_map/all_gather | solution.py:189
  91.7 0.9 fusion.63
  92.7 1.3 fusion.12
  93.9 1.7 convolution_convert_fusion
  95.7 0.8 reshape.274
  96.4 3.5 %all-to-all-start.5 = ((bf16[16,5,1024]{2,1,0:T(8,128)(2,1)}), bf16[16,5,1024]{2,1,0:T(8,128)(2,1)S(1)}, u32[]{:S(2)}, u32[]{:S(2)}) async-start(bf16[16,5,1024]{2,1,0:T(8,128)(2,1)} %reshape.274), calls=%async_computation.5 | async-start | bytes 524288 | tf_op jit(solution)/shard_map/all_to_all | solution.py:186
  100.0 2.3 %fusion.4 = f32[64,1024]{1,0:T(8,128)} fusion(bf16[256,1024]{1,0:T(8,128)(2,1)S(1)} %copy-done.1, bf16[64,1024]{1,0:T(8,128)(2,1)S(1)} %reshape.292, bf16[256,1024]{1,0:T(8,128)(2,1)} %param.45, f32[64,256]{1,0:T(8,128)S(1)} %copy-done.5), kind=kOutput, calls=%fused_computation.10 | convolution fusion | flops 67207168 | bytes 1507328 | tf_op jit(solution)/shard_map/dot_general | solution.py:195
  102.4 7.5 %all-to-all-done.5 = bf16[16,5,1024]{2,1,0:T(8,128)(2,1)S(1)} async-done(((bf16[16,5,1024]{2,1,0:T(8,128)(2,1)}), bf16[16,5,1024]{2,1,0:T(8,128)(2,1)S(1)}, u32[]{:S(2)}, u32[]{:S(2)}) %all-to-all-start.5) | async-done | bytes 163872 | tf_op jit(solution)/shard_map/all_to_all | solution.py:186
  110.0 0.6 gather_fusion
  110.8 84.8 %all-reduce.4.cloned.1.call-done = f32[64,1024]{1,0:T(8,128)} async-done(((f32[64,1024]{1,0:T(8,128)}), f32[64,1024]{1,0:T(8,128)}) %all-reduce.4.cloned.1.call-update) | async-done | bytes 262160
  195.6 0.9 multiply_reduce_fusion.2
  196.6 1.4 fusion.38
  (75 shorter events, 2.5 us)
Async XLA Ops:
  7.2 35.4 %copy-start = (bf16[4,1024,256]{2,1,0:T(8,128)(2,1)S(1)}, bf16[4,1024,256]{2,1,0:T(8,128)(2,1)}, u32[]{:S(2)}) copy-start(bf16[4,1024,256]{2,1,0:T(8,128)(2,1)} %param.26) | copy-start | bytes 6291460
  7.2 36.0 %copy-start.4 = (bf16[4,32,1024]{2,1,0:T(8,128)(2,1)S(1)}, bf16[4,32,1024]{2,1,0:T(8,128)(2,1)}, u32[]{:S(2)}) copy-start(bf16[4,32,1024]{2,1,0:T(8,128)(2,1)} %param.27) | copy-start | bytes 786436
  16.4 11.7 %all-to-all-start.1 = ((bf16[2,2,256]{2,1,0:T(2,128)(2,1)}), bf16[2,2,256]{2,1,0:T(2,128)(2,1)S(1)}, u32[]{:S(2)}, u32[]{:S(2)}) async-start(bf16[2,2,256]{2,1,0:T(2,128)(2,1)} %reshape.295), calls=%async_computation.1 | async-start | bytes 4096 | tf_op jit(solution)/shard_map/all_to_all | solution.py:141
  28.1 7.1 %all-to-all-start.2 = ((f32[2,4,128]{2,1,0:T(4,128)}), f32[2,4,128]{2,1,0:T(4,128)S(1)}, u32[]{:S(2)}, u32[]{:S(2)}) async-start(f32[2,4,128]{2,1,0:T(4,128)} %bitcast.9), calls=%async_computation.2 | async-start | bytes 8192 | tf_op jit(solution)/shard_map/all_to_all | solution.py:130
  35.2 7.1 %all-to-all-start = ((bf16[8,4,256]{2,1,0:T(4,128)(2,1)}), bf16[8,4,256]{2,1,0:T(4,128)(2,1)S(1)}, u32[]{:S(2)}, u32[]{:S(2)}) async-start(bf16[8,4,256]{2,1,0:T(4,128)(2,1)} %copy.49), calls=%async_computation | async-start | bytes 32768 | tf_op jit(solution)/shard_map/all_to_all | solution.py:140
  42.6 5.7 %copy-start.14 = (u32[32]{0:T(128)S(1)}, u32[32]{0:T(128)}, u32[]{:S(2)}) copy-start(u32[32]{0:T(128)} %constant.51) | copy-start | bytes 388
  43.2 8.7 %copy-start.6 = (bf16[4,256,64]{1,2,0:T(8,128)(2,1)S(1)}, bf16[4,256,64]{1,2,0:T(8,128)(2,1)}, u32[]{:S(2)}) copy-start(bf16[4,256,64]{1,2,0:T(8,128)(2,1)} %param.37) | copy-start | bytes 393220
  43.2 9.0 %copy-start.2 = (bf16[256,1024]{1,0:T(8,128)(2,1)S(1)}, bf16[256,1024]{1,0:T(8,128)(2,1)}, u32[]{:S(2)}) copy-start(bf16[256,1024]{1,0:T(8,128)(2,1)} %param.38) | copy-start | bytes 1572868
  43.2 16.0 %copy-start.7 = (bf16[4,1024]{1,0:T(4,128)(2,1)S(1)}, bf16[4,1024]{1,0:T(4,128)(2,1)}, u32[]{:S(2)}) copy-start(bf16[4,1024]{1,0:T(4,128)(2,1)} %param.24) | copy-start | bytes 24580
  43.2 16.0 %copy-start.10 = (f32[1024]{0:T(1024)S(1)}, f32[1024]{0:T(1024)}, u32[]{:S(2)}) copy-start(f32[1024]{0:T(1024)} %param.30) | copy-start | bytes 12292
  43.3 16.2 %copy-start.8 = (f32[1024]{0:T(1024)S(1)}, f32[1024]{0:T(1024)}, u32[]{:S(2)}) copy-start(f32[1024]{0:T(1024)} %param.47) | copy-start | bytes 12292
  43.3 16.2 %copy-start.9 = (f32[1024]{0:T(1024)S(1)}, f32[1024]{0:T(1024)}, u32[]{:S(2)}) copy-start(f32[1024]{0:T(1024)} %param.31) | copy-start | bytes 12292
  43.8 47.9 %copy-start.3 = (bf16[256,1024]{1,0:T(8,128)(2,1)S(1)}, bf16[256,1024]{1,0:T(8,128)(2,1)}, u32[]{:S(2)}) copy-start(bf16[256,1024]{1,0:T(8,128)(2,1)} %param.44) | copy-start | bytes 1572868
  44.8 7.1 %all-to-all-start.3 = ((bf16[4,8,256]{2,0,1:T(4,128)(2,1)}), bf16[4,8,256]{2,0,1:T(4,128)(2,1)S(1)}, u32[]{:S(2)}, u32[]{:S(2)}) async-start(bf16[4,8,256]{2,0,1:T(4,128)(2,1)} %copy.55), calls=%async_computation.3 | async-start | bytes 32768 | tf_op jit(solution)/shard_map/all_to_all | solution.py:154
  61.2 31.4 %all-to-all-start.4 = ((bf16[16,5,1024]{2,1,0:T(8,128)(2,1)}), bf16[16,5,1024]{2,1,0:T(8,128)(2,1)S(1)}, u32[]{:S(2)}, u32[]{:S(2)}) async-start(bf16[16,5,1024]{2,1,0:T(8,128)(2,1)} %reshape.272), calls=%async_computation.4 | async-start | bytes 524288 | tf_op jit(solution)/shard_map/all_to_all | solution.py:181
  91.7 8.4 %copy-start.1 = (bf16[256,1024]{1,0:T(8,128)(2,1)S(1)}, bf16[256,1024]{1,0:T(8,128)(2,1)}, u32[]{:S(2)}) copy-start(bf16[256,1024]{1,0:T(8,128)(2,1)} %param.46) | copy-start | bytes 1572868
  92.6 7.5 %copy-start.5 = (f32[64,256]{1,0:T(8,128)S(1)}, f32[64,256]{1,0:T(8,128)}, u32[]{:S(2)}) copy-start(f32[64,256]{1,0:T(8,128)} %fusion.63) | copy-start | bytes 196612
  93.9 8.5 %copy-start.13 = (f32[4]{0:T(128)S(1)}, f32[4]{0:T(128)}, u32[]{:S(2)}) copy-start(f32[4]{0:T(128)} %get-tuple-element.3) | copy-start | bytes 52
  95.7 15.0 %copy-start.12 = (f32[4,6]{1,0:T(4,128)S(1)}, f32[4,6]{1,0:T(4,128)}, u32[]{:S(2)}) copy-start(f32[4,6]{1,0:T(4,128)} %param.40) | copy-start | bytes 292
  95.7 100.9 %copy-start.11 = (f32[1024]{0:T(1024)S(1)}, f32[1024]{0:T(1024)}, u32[]{:S(2)}) copy-start(f32[1024]{0:T(1024)} %param.32) | copy-start | bytes 12292
  96.4 13.5 %all-to-all-start.5 = ((bf16[16,5,1024]{2,1,0:T(8,128)(2,1)}), bf16[16,5,1024]{2,1,0:T(8,128)(2,1)S(1)}, u32[]{:S(2)}, u32[]{:S(2)}) async-start(bf16[16,5,1024]{2,1,0:T(8,128)(2,1)} %reshape.274), calls=%async_computation.5 | async-start | bytes 524288 | tf_op jit(solution)/shard_map/all_to_all | solution.py:186
  100.0 95.7 %all-reduce.4.cloned.1.call-start = ((), (), s32[]{:S(2)}) async-start(), calls=%async_computation.6 | async-start | bytes 524288
Sparse Core Ops, SparseCore 0:
  104.2 91.4 all-reduce.3
where the time goes:
time: 206 us; the launch traced here: 205 us
  waiting for transfers between devices  101 us (49%)
  blocking collectives  34.1 us (17%)
  starting transfers between devices  23 us (11%)
  between operations  15.6 us (8%)
  matrix products  13.3 us (6%)
  other arithmetic  10.3 us (5%)
  local copies, waits for them, and re-layouts  7.86 us (4%)
    unnamed x2, waiting for transfers between devices  84.8 us
    all_gather x1, blocking collectives, shards(): piece_rows = lax.all_gather(ffn_in, 'ep', axis=0, tiled=True)  22.1 us
    all_to_all x1, waiting for transfers between devices, shards(): lax.all_to_all(result, 'ep', split_axis=0, concat_axis=0, tiled=True)  7.54 us
    unnamed x1, blocking collectives  6.72 us
    all_to_all x1, starting transfers between devices, shards(): lax.all_to_all(outgoing, 'ep', split_axis=0, concat_axis=0, tiled=True)  6.39 us
    all_gather x1, blocking collectives, shards(): group_hidden = lax.all_gather(hidden, 'tp', axis=0, tiled=True)  5.27 us
  transfers between devices with their start and end apart: 7, of which 5 were waited for; matrix products, arithmetic and copies ran while one was open for 8% of the time, Pallas kernels for 0%

commit v1 on v0

--- a/solution.py
+++ b/solution.py
@@ -6,6 +6,17 @@
 epsilon = 1e-06
 rope_base = 10000.0
 negative = -1e30
+
+
+def in_blocks(value, dim, size):
+    before, after = (value.shape[:dim], value.shape[dim + 1 :])
+    return jnp.moveaxis(value.reshape(*before, size, -1, *after), dim, 0)
+
+
+def in_order(parts, dim):
+    lengths = list(parts.shape[1:])
+    lengths[dim] *= parts.shape[0]
+    return jnp.moveaxis(parts, 0, dim).reshape(lengths)
 
 
 def normalize(values, gain_vec):
@@ -183,7 +194,14 @@
         up_w,
         down_w,
     )
-    returned = lax.all_to_all(result, "ep", split_axis=0, concat_axis=0, tiled=True)
+    length, index = (lax.axis_size("ep"), lax.axis_index("ep"))
+    pieces = in_blocks(result, 0, length)
+    outs = [pieces[index]]
+    for step in range(1, length):
+        sent = pieces[index ^ step]
+        outs.append(lax.ppermute(sent, "ep", [(i, i ^ step) for i in range(length)]))
+    pieces = jnp.stack(outs)[index ^ jnp.arange(length)]
+    returned = in_order(pieces, 0)
     picked = returned.reshape(ep_count * capacity, model_width)[slot_index].astype(jnp.float32)
     routed = jnp.sum(route_weights[..., None] * picked, axis=1)
     piece_rows = lax.all_gather(ffn_in, "ep", axis=0, tiled=True)

time: 206 us -> 196 us (0.951)
  waiting for transfers between devices: 101 us -> 69.4 us
  starting transfers between devices: 23 us -> 39.9 us
  blocking collectives: 34.1 us -> 36.3 us
    unnamed x2, waiting for transfers between devices: 84.8 us -> 60.1 us
    ppermute x0 -> x15, starting transfers between devices: none -> 20.4 us  [shards(): lax.ppermute(sent, 'ep', [(i, i ^ step) for i in range(length)])]
    all_to_all x1 -> x0, waiting for transfers between devices: 7.54 us -> none  [shards(): lax.all_to_all(result, 'ep', split_axis=0, concat_axis=0, tiled=True)]
    all_to_all x1 -> x0, starting transfers between devices: 3.53 us -> none  [shards(): lax.all_to_all(result, 'ep', split_axis=0, concat_axis=0, tiled=True)]
    ppermute x0 -> x15, waiting for transfers between devices: none -> 2.42 us  [shards(): lax.ppermute(sent, 'ep', [(i, i ^ step) for i in range(length)])]
  transfers between devices with their start and end apart: 7 -> 21, of which waited for: 5 -> 6; matrix products, arithmetic and copies ran while one was open for 8% -> 11% of each run, Pallas kernels for 0% -> 0%
where the time goes in v1:
time: 196 us; the launch traced here: 195 us
  waiting for transfers between devices  69.4 us (35%)
  starting transfers between devices  39.9 us (20%)
  blocking collectives  36.3 us (19%)
  between operations  15.9 us (8%)
  matrix products  15.2 us (8%)
  other arithmetic  10.3 us (5%)
  local copies, waits for them, and re-layouts  8.11 us (4%)
    unnamed x2, waiting for transfers between devices  60.1 us
    all_gather x1, blocking collectives, shards(): piece_rows = lax.all_gather(ffn_in, 'ep', axis=0, tiled=True)  23.6 us
    ppermute x15, starting transfers between devices, shards(): lax.ppermute(sent, 'ep', [(i, i ^ step) for i in range(length)])  20.4 us
    unnamed x1, blocking collectives  7.5 us
    all_to_all x1, starting transfers between devices, shards(): lax.all_to_all(outgoing, 'ep', split_axis=0, concat_axis=0, tiled=True)  6.39 us
    all_gather x1, blocking collectives, shards(): group_hidden = lax.all_gather(hidden, 'tp', axis=0, tiled=True)  5.27 us
  transfers between devices with their start and end apart: 21, of which 6 were waited for; matrix products, arithmetic and copies ran while one was open for 11% of the time, Pallas kernels for 0%

profile of v1, /device:TPU:0, one launch (start us, length us, event | category | flops | bytes accessed | tf_op | source)
XLA Modules:
  0.0 195.2 jit_solution(4490124801480925766)
XLA Ops:
  7.2 1.0 fusion.31
  8.2 0.8 fusion.55
  9.0 5.3 %all-gather = bf16[2,4,1024]{2,1,0:T(4,128)(2,1)S(1)} all-gather(bf16[1,4,1024]{2,1,0:T(4,128)(2,1)S(1)} %fusion.55), channel_id=1, replica_groups=mesh['ep'=16,'tp'=2] {'tp'}, dimensions={0}, use_global_device_ids=true | all-gather | bytes 24576 | tf_op jit(solution)/shard_map/all_gather | solution.py:139
  14.2 1.3 convolution_convert_fusion.5
  15.8 0.7 reshape.314
  16.4 3.3 %all-to-all-start.1 = ((bf16[2,2,256]{2,1,0:T(2,128)(2,1)}), bf16[2,2,256]{2,1,0:T(2,128)(2,1)S(1)}, u32[]{:S(2)}, u32[]{:S(2)}) async-start(bf16[2,2,256]{2,1,0:T(2,128)(2,1)} %reshape.314), calls=%async_computation.1 | async-start | bytes 4096 | tf_op jit(solution)/shard_map/all_to_all | solution.py:152
  19.8 0.7 convert_element_type.152
  20.4 0.7 iota_compare_fusion
  21.1 1.1 fusion.53
  22.2 1.7 fusion.63
  23.9 0.8 eq.28
  24.9 0.7 compare_select_fusion
  25.8 1.0 fusion.6
  27.0 0.6 fusion.58
  27.6 0.6 copy.49
  28.3 3.3 %all-to-all-start.2 = ((f32[2,4,128]{2,1,0:T(4,128)}), f32[2,4,128]{2,1,0:T(4,128)S(1)}, u32[]{:S(2)}, u32[]{:S(2)}) async-start(f32[2,4,128]{2,1,0:T(4,128)} %bitcast.9), calls=%async_computation.2 | async-start | bytes 8192 | tf_op jit(solution)/shard_map/all_to_all | solution.py:141
  31.9 3.5 %all-to-all-done.2 = f32[2,4,128]{2,1,0:T(4,128)S(1)} async-done(((f32[2,4,128]{2,1,0:T(4,128)}), f32[2,4,128]{2,1,0:T(4,128)S(1)}, u32[]{:S(2)}, u32[]{:S(2)}) %all-to-all-start.2) | async-done | bytes 4128 | tf_op jit(solution)/shard_map/all_to_all | solution.py:141
  35.4 3.2 %all-to-all-start = ((bf16[8,4,256]{2,1,0:T(4,128)(2,1)}), bf16[8,4,256]{2,1,0:T(4,128)(2,1)S(1)}, u32[]{:S(2)}, u32[]{:S(2)}) async-start(bf16[8,4,256]{2,1,0:T(4,128)(2,1)} %copy.49), calls=%async_computation | async-start | bytes 32768 | tf_op jit(solution)/shard_map/all_to_all | solution.py:151
  38.7 1.3 fusion.59
  40.1 2.4 %all-to-all-done = bf16[8,4,256]{2,1,0:T(4,128)(2,1)S(1)} async-done(((bf16[8,4,256]{2,1,0:T(4,128)(2,1)}), bf16[8,4,256]{2,1,0:T(4,128)(2,1)S(1)}, u32[]{:S(2)}, u32[]{:S(2)}) %all-to-all-start) | async-done | bytes 16416 | tf_op jit(solution)/shard_map/all_to_all | solution.py:151
  42.8 0.6 fusion.62
  44.5 0.6 copy.55
  45.1 3.2 %all-to-all-start.3 = ((bf16[4,8,256]{2,0,1:T(4,128)(2,1)}), bf16[4,8,256]{2,0,1:T(4,128)(2,1)S(1)}, u32[]{:S(2)}, u32[]{:S(2)}) async-start(bf16[4,8,256]{2,0,1:T(4,128)(2,1)} %copy.55), calls=%async_computation.3 | async-start | bytes 32768 | tf_op jit(solution)/shard_map/all_to_all | solution.py:165
  49.0 0.7 dynamic-slice.2
  51.1 1.1 all-to-all-done.3
  52.4 1.2 convolution_convert_fusion.3
  53.7 7.5 %all-reduce = bf16[8,1024]{1,0:T(8,128)(2,1)S(1)} all-reduce(bf16[8,1024]{1,0:T(8,128)(2,1)S(1)} %convolution_convert_fusion.3), channel_id=2, replica_groups=mesh['ep'=16,'tp'=2] {'tp'}, use_global_device_ids=true, to_apply=%region_6.7.clone | all-reduce | flops 8192 | bytes 32768
  61.5 0.7 multiply_reduce_fusion.3
  62.5 0.8 reshape.282
  63.3 6.4 %all-to-all-start.4 = ((bf16[16,5,1024]{2,1,0:T(8,128)(2,1)}), bf16[16,5,1024]{2,1,0:T(8,128)(2,1)S(1)}, u32[]{:S(2)}, u32[]{:S(2)}) async-start(bf16[16,5,1024]{2,1,0:T(8,128)(2,1)} %reshape.282), calls=%async_computation.4 | async-start | bytes 524288 | tf_op jit(solution)/shard_map/all_to_all | solution.py:192
  69.7 23.6 %all-gather.1 = bf16[16,4,1024]{2,1,0:T(4,128)(2,1)} all-gather(bf16[1,4,1024]{2,1,0:T(4,128)(2,1)S(1)} %bitcast.140), channel_id=1, replica_groups=mesh['ep'=16,'tp'=2] {'ep'}, dimensions={0}, use_global_device_ids=true | all-gather | bytes 139264 | tf_op jit(solution)/shard_map/all_gather | solution.py:207
  93.3 0.9 reshape.311
  94.2 2.0 fusion.64
  96.2 2.1 %fusion.4 = f32[64,1024]{1,0:T(8,128)} fusion(bf16[256,1024]{1,0:T(8,128)(2,1)S(1)} %copy-done.1, bf16[64,1024]{1,0:T(8,128)(2,1)S(1)} %reshape.311, bf16[256,1024]{1,0:T(8,128)(2,1)S(1)} %copy-done.2, f32[64,256]{1,0:T(8,128)} %fusion.64), kind=kOutput, calls=%fused_computation.11 | convolution fusion | flops 67207168 | bytes 1507328 | tf_op jit(solution)/shard_map/dot_general | solution.py:213
  98.4 1.3 fusion.12
  99.7 1.7 convolution_convert_fusion
  102.5 1.1 collective-permute-start.2
  103.6 2.0 %collective-permute-start.4 = (bf16[1,5,1024]{2,1,0:T(8,128)(2,1)S(1)}, bf16[1,5,1024]{2,1,0:T(8,128)(2,1)S(1)}, u32[]{:S(2)}, u32[]{:S(2)}) collective-permute-start(bf16[1,5,1024]{2,1,0:T(8,128)(2,1)S(1)} %get-tuple-element.23), channel_id=1, source_target_pairs={{0,10},{2,8},{4,14},{6,12},{8,2},{10,0},{12,6},{14,4},{16,26},{18,... | collective-permute-start | bytes 30728 | tf_op jit(solution)/shard_map/ppermute | solution.py:202
  105.9 2.1 %collective-permute-start.6 = (bf16[1,5,1024]{2,1,0:T(8,128)(2,1)S(1)}, bf16[1,5,1024]{2,1,0:T(8,128)(2,1)S(1)}, u32[]{:S(2)}, u32[]{:S(2)}) collective-permute-start(bf16[1,5,1024]{2,1,0:T(8,128)(2,1)S(1)} %get-tuple-element.21), channel_id=1, source_target_pairs={{0,14},{2,12},{4,10},{6,8},{8,6},{10,4},{12,2},{14,0},{16,30},{18,... | collective-permute-start | bytes 30728 | tf_op jit(solution)/shard_map/ppermute | solution.py:202
  108.0 2.9 %collective-permute-start.8 = (bf16[1,5,1024]{2,1,0:T(8,128)(2,1)S(1)}, bf16[1,5,1024]{2,1,0:T(8,128)(2,1)S(1)}, u32[]{:S(2)}, u32[]{:S(2)}) collective-permute-start(bf16[1,5,1024]{2,1,0:T(8,128)(2,1)S(1)} %get-tuple-element.19), channel_id=1, source_target_pairs={{0,18},{2,16},{4,22},{6,20},{8,26},{10,24},{12,30},{14,28},{16,2},... | collective-permute-start | bytes 30728 | tf_op jit(solution)/shard_map/ppermute | solution.py:202
  111.1 3.1 %collective-permute-start.10 = (bf16[1,5,1024]{2,1,0:T(8,128)(2,1)S(1)}, bf16[1,5,1024]{2,1,0:T(8,128)(2,1)S(1)}, u32[]{:S(2)}, u32[]{:S(2)}) collective-permute-start(bf16[1,5,1024]{2,1,0:T(8,128)(2,1)S(1)} %get-tuple-element.17), channel_id=1, source_target_pairs={{0,22},{2,20},{4,18},{6,16},{8,30},{10,28},{12,26},{14,24},{16,6},... | collective-permute-start | bytes 30728 | tf_op jit(solution)/shard_map/ppermute | solution.py:202
  114.2 3.7 %collective-permute-start.12 = (bf16[1,5,1024]{2,1,0:T(8,128)(2,1)S(1)}, bf16[1,5,1024]{2,1,0:T(8,128)(2,1)S(1)}, u32[]{:S(2)}, u32[]{:S(2)}) collective-permute-start(bf16[1,5,1024]{2,1,0:T(8,128)(2,1)S(1)} %get-tuple-element.15), channel_id=1, source_target_pairs={{0,26},{2,24},{4,30},{6,28},{8,18},{10,16},{12,22},{14,20},{16,10}... | collective-permute-start | bytes 30728 | tf_op jit(solution)/shard_map/ppermute | solution.py:202
  118.4 3.8 %collective-permute-start.14 = (bf16[1,5,1024]{2,1,0:T(8,128)(2,1)S(1)}, bf16[1,5,1024]{2,1,0:T(8,128)(2,1)S(1)}, u32[]{:S(2)}, u32[]{:S(2)}) collective-permute-start(bf16[1,5,1024]{2,1,0:T(8,128)(2,1)S(1)} %get-tuple-element.13), channel_id=1, source_target_pairs={{0,30},{2,28},{4,26},{6,24},{8,22},{10,20},{12,18},{14,16},{16,14}... | collective-permute-start | bytes 30728 | tf_op jit(solution)/shard_map/ppermute | solution.py:202
  122.3 2.2 %collective-permute-done.13 = bf16[1,5,1024]{2,1,0:T(8,128)(2,1)S(1)} collective-permute-done((bf16[1,5,1024]{2,1,0:T(8,128)(2,1)S(1)}, bf16[1,5,1024]{2,1,0:T(8,128)(2,1)S(1)}, u32[]{:S(2)}, u32[]{:S(2)}) %collective-permute-start.13) | collective-permute-done | bytes 10272 | tf_op jit(solution)/shard_map/ppermute | solution.py:202
  125.2 0.6 gather_fusion.1
  125.9 60.0 %all-reduce.4.cloned.1.call-done = f32[64,1024]{1,0:T(8,128)} async-done(((f32[64,1024]{1,0:T(8,128)}), f32[64,1024]{1,0:T(8,128)}) %all-reduce.4.cloned.1.call-update) | async-done | bytes 262160
  186.0 0.9 multiply_reduce_fusion.2
  186.9 1.4 fusion.38
  (120 shorter events, 7.1 us)
Async XLA Ops:
  7.2 35.6 %copy-start = (bf16[4,1024,256]{2,1,0:T(8,128)(2,1)S(1)}, bf16[4,1024,256]{2,1,0:T(8,128)(2,1)}, u32[]{:S(2)}) copy-start(bf16[4,1024,256]{2,1,0:T(8,128)(2,1)} %param.26) | copy-start | bytes 6291460
  7.2 36.2 %copy-start.3 = (bf16[4,32,1024]{2,1,0:T(8,128)(2,1)S(1)}, bf16[4,32,1024]{2,1,0:T(8,128)(2,1)}, u32[]{:S(2)}) copy-start(bf16[4,32,1024]{2,1,0:T(8,128)(2,1)} %param.27) | copy-start | bytes 786436
  16.4 11.9 %all-to-all-start.1 = ((bf16[2,2,256]{2,1,0:T(2,128)(2,1)}), bf16[2,2,256]{2,1,0:T(2,128)(2,1)S(1)}, u32[]{:S(2)}, u32[]{:S(2)}) async-start(bf16[2,2,256]{2,1,0:T(2,128)(2,1)} %reshape.314), calls=%async_computation.1 | async-start | bytes 4096 | tf_op jit(solution)/shard_map/all_to_all | solution.py:152
  28.3 7.1 %all-to-all-start.2 = ((f32[2,4,128]{2,1,0:T(4,128)}), f32[2,4,128]{2,1,0:T(4,128)S(1)}, u32[]{:S(2)}, u32[]{:S(2)}) async-start(f32[2,4,128]{2,1,0:T(4,128)} %bitcast.9), calls=%async_computation.2 | async-start | bytes 8192 | tf_op jit(solution)/shard_map/all_to_all | solution.py:141
  35.4 7.1 %all-to-all-start = ((bf16[8,4,256]{2,1,0:T(4,128)(2,1)}), bf16[8,4,256]{2,1,0:T(4,128)(2,1)S(1)}, u32[]{:S(2)}, u32[]{:S(2)}) async-start(bf16[8,4,256]{2,1,0:T(4,128)(2,1)} %copy.49), calls=%async_computation | async-start | bytes 32768 | tf_op jit(solution)/shard_map/all_to_all | solution.py:151
  43.4 5.0 %copy-start.13 = (u32[32]{0:T(128)S(1)}, u32[32]{0:T(128)}, u32[]{:S(2)}) copy-start(u32[32]{0:T(128)} %constant.91) | copy-start | bytes 388
  43.4 5.6 %copy-start.12 = (u32[32]{0:T(128)S(1)}, u32[32]{0:T(128)}, u32[]{:S(2)}) copy-start(u32[32]{0:T(128)} %constant.95) | copy-start | bytes 388
  43.4 8.8 %copy-start.4 = (bf16[4,256,64]{1,2,0:T(8,128)(2,1)S(1)}, bf16[4,256,64]{1,2,0:T(8,128)(2,1)}, u32[]{:S(2)}) copy-start(bf16[4,256,64]{1,2,0:T(8,128)(2,1)} %param.37) | copy-start | bytes 393220
  43.5 17.8 %copy-start.5 = (bf16[4,1024]{1,0:T(4,128)(2,1)S(1)}, bf16[4,1024]{1,0:T(4,128)(2,1)}, u32[]{:S(2)}) copy-start(bf16[4,1024]{1,0:T(4,128)(2,1)} %param.24) | copy-start | bytes 24580
  43.5 17.8 %copy-start.8 = (f32[1024]{0:T(1024)S(1)}, f32[1024]{0:T(1024)}, u32[]{:S(2)}) copy-start(f32[1024]{0:T(1024)} %param.30) | copy-start | bytes 12292
  43.5 18.0 %copy-start.6 = (f32[1024]{0:T(1024)S(1)}, f32[1024]{0:T(1024)}, u32[]{:S(2)}) copy-start(f32[1024]{0:T(1024)} %param.47) | copy-start | bytes 12292
  43.5 18.0 %copy-start.7 = (f32[1024]{0:T(1024)S(1)}, f32[1024]{0:T(1024)}, u32[]{:S(2)}) copy-start(f32[1024]{0:T(1024)} %param.31) | copy-start | bytes 12292
  44.4 51.7 %copy-start.1 = (bf16[256,1024]{1,0:T(8,128)(2,1)S(1)}, bf16[256,1024]{1,0:T(8,128)(2,1)}, u32[]{:S(2)}) copy-start(bf16[256,1024]{1,0:T(8,128)(2,1)} %param.46) | copy-start | bytes 1572868
  44.5 51.7 %copy-start.2 = (bf16[256,1024]{1,0:T(8,128)(2,1)S(1)}, bf16[256,1024]{1,0:T(8,128)(2,1)}, u32[]{:S(2)}) copy-start(bf16[256,1024]{1,0:T(8,128)(2,1)} %param.45) | copy-start | bytes 1572868
  45.1 7.1 %all-to-all-start.3 = ((bf16[4,8,256]{2,0,1:T(4,128)(2,1)}), bf16[4,8,256]{2,0,1:T(4,128)(2,1)S(1)}, u32[]{:S(2)}, u32[]{:S(2)}) async-start(bf16[4,8,256]{2,0,1:T(4,128)(2,1)} %copy.55), calls=%async_computation.3 | async-start | bytes 32768 | tf_op jit(solution)/shard_map/all_to_all | solution.py:165
  63.3 35.0 %all-to-all-start.4 = ((bf16[16,5,1024]{2,1,0:T(8,128)(2,1)}), bf16[16,5,1024]{2,1,0:T(8,128)(2,1)S(1)}, u32[]{:S(2)}, u32[]{:S(2)}) async-start(bf16[16,5,1024]{2,1,0:T(8,128)(2,1)} %reshape.282), calls=%async_computation.4 | async-start | bytes 524288 | tf_op jit(solution)/shard_map/all_to_all | solution.py:192
  69.7 116.3 %all-reduce.4.cloned.1.call-start = ((), (), s32[]{:S(2)}) async-start(), calls=%async_computation.5 | async-start | bytes 524288
  98.3 3.7 %copy-start.11 = (f32[4]{0:T(128)S(1)}, f32[4]{0:T(128)}, u32[]{:S(2)}) copy-start(f32[4]{0:T(128)} %get-tuple-element.3) | copy-start | bytes 52
  99.7 26.1 %copy-start.10 = (f32[4,6]{1,0:T(4,128)S(1)}, f32[4,6]{1,0:T(4,128)}, u32[]{:S(2)}) copy-start(f32[4,6]{1,0:T(4,128)} %param.40) | copy-start | bytes 292
  99.7 87.3 %copy-start.9 = (f32[1024]{0:T(1024)S(1)}, f32[1024]{0:T(1024)}, u32[]{:S(2)}) copy-start(f32[1024]{0:T(1024)} %param.32) | copy-start | bytes 12292
  101.6 4.0 %collective-permute-start = (bf16[1,5,1024]{2,1,0:T(8,128)(2,1)S(1)}, bf16[1,5,1024]{2,1,0:T(8,128)(2,1)S(1)}, u32[]{:S(2)}, u32[]{:S(2)}) collective-permute-start(bf16[1,5,1024]{2,1,0:T(8,128)(2,1)S(1)} %get-tuple-element.27), channel_id=1, source_target_pairs={{0,2},{2,0},{4,6},{6,4},{8,10},{10,8},{12,14},{14,12},{16,18},{18,... | collective-permute-start | bytes 30728 | tf_op jit(solution)/shard_map/ppermute | solution.py:202
  102.0 3.9 %collective-permute-start.1 = (bf16[1,5,1024]{2,1,0:T(8,128)(2,1)S(1)}, bf16[1,5,1024]{2,1,0:T(8,128)(2,1)S(1)}, u32[]{:S(2)}, u32[]{:S(2)}) collective-permute-start(bf16[1,5,1024]{2,1,0:T(8,128)(2,1)S(1)} %get-tuple-element.26), channel_id=1, source_target_pairs={{0,4},{2,6},{4,0},{6,2},{8,12},{10,14},{12,8},{14,10},{16,20},{18,... | collective-permute-start | bytes 30728 | tf_op jit(solution)/shard_map/ppermute | solution.py:202
  102.5 5.5 %collective-permute-start.2 = (bf16[1,5,1024]{2,1,0:T(8,128)(2,1)S(1)}, bf16[1,5,1024]{2,1,0:T(8,128)(2,1)S(1)}, u32[]{:S(2)}, u32[]{:S(2)}) collective-permute-start(bf16[1,5,1024]{2,1,0:T(8,128)(2,1)S(1)} %get-tuple-element.25), channel_id=1, source_target_pairs={{0,6},{2,4},{4,2},{6,0},{8,14},{10,12},{12,10},{14,8},{16,22},{18,... | collective-permute-start | bytes 30728 | tf_op jit(solution)/shard_map/ppermute | solution.py:202
  103.6 4.4 %collective-permute-start.3 = (bf16[1,5,1024]{2,1,0:T(8,128)(2,1)S(1)}, bf16[1,5,1024]{2,1,0:T(8,128)(2,1)S(1)}, u32[]{:S(2)}, u32[]{:S(2)}) collective-permute-start(bf16[1,5,1024]{2,1,0:T(8,128)(2,1)S(1)} %get-tuple-element.24), channel_id=1, source_target_pairs={{0,8},{2,10},{4,12},{6,14},{8,0},{10,2},{12,4},{14,6},{16,24},{18,... | collective-permute-start | bytes 30728 | tf_op jit(solution)/shard_map/ppermute | solution.py:202
  103.6 7.3 %collective-permute-start.4 = (bf16[1,5,1024]{2,1,0:T(8,128)(2,1)S(1)}, bf16[1,5,1024]{2,1,0:T(8,128)(2,1)S(1)}, u32[]{:S(2)}, u32[]{:S(2)}) collective-permute-start(bf16[1,5,1024]{2,1,0:T(8,128)(2,1)S(1)} %get-tuple-element.23), channel_id=1, source_target_pairs={{0,10},{2,8},{4,14},{6,12},{8,2},{10,0},{12,6},{14,4},{16,26},{18,... | collective-permute-start | bytes 30728 | tf_op jit(solution)/shard_map/ppermute | solution.py:202
  105.6 5.5 %collective-permute-start.5 = (bf16[1,5,1024]{2,1,0:T(8,128)(2,1)S(1)}, bf16[1,5,1024]{2,1,0:T(8,128)(2,1)S(1)}, u32[]{:S(2)}, u32[]{:S(2)}) collective-permute-start(bf16[1,5,1024]{2,1,0:T(8,128)(2,1)S(1)} %get-tuple-element.22), channel_id=1, source_target_pairs={{0,12},{2,14},{4,8},{6,10},{8,4},{10,6},{12,0},{14,2},{16,28},{18,... | collective-permute-start | bytes 30728 | tf_op jit(solution)/shard_map/ppermute | solution.py:202
  105.9 8.3 %collective-permute-start.6 = (bf16[1,5,1024]{2,1,0:T(8,128)(2,1)S(1)}, bf16[1,5,1024]{2,1,0:T(8,128)(2,1)S(1)}, u32[]{:S(2)}, u32[]{:S(2)}) collective-permute-start(bf16[1,5,1024]{2,1,0:T(8,128)(2,1)S(1)} %get-tuple-element.21), channel_id=1, source_target_pairs={{0,14},{2,12},{4,10},{6,8},{8,6},{10,4},{12,2},{14,0},{16,30},{18,... | collective-permute-start | bytes 30728 | tf_op jit(solution)/shard_map/ppermute | solution.py:202
  108.0 6.3 %collective-permute-start.7 = (bf16[1,5,1024]{2,1,0:T(8,128)(2,1)S(1)}, bf16[1,5,1024]{2,1,0:T(8,128)(2,1)S(1)}, u32[]{:S(2)}, u32[]{:S(2)}) collective-permute-start(bf16[1,5,1024]{2,1,0:T(8,128)(2,1)S(1)} %get-tuple-element.20), channel_id=1, source_target_pairs={{0,16},{2,18},{4,20},{6,22},{8,24},{10,26},{12,28},{14,30},{16,0},... | collective-permute-start | bytes 30728 | tf_op jit(solution)/shard_map/ppermute | solution.py:202
  108.0 10.0 %collective-permute-start.8 = (bf16[1,5,1024]{2,1,0:T(8,128)(2,1)S(1)}, bf16[1,5,1024]{2,1,0:T(8,128)(2,1)S(1)}, u32[]{:S(2)}, u32[]{:S(2)}) collective-permute-start(bf16[1,5,1024]{2,1,0:T(8,128)(2,1)S(1)} %get-tuple-element.19), channel_id=1, source_target_pairs={{0,18},{2,16},{4,22},{6,20},{8,26},{10,24},{12,30},{14,28},{16,2},... | collective-permute-start | bytes 30728 | tf_op jit(solution)/shard_map/ppermute | solution.py:202
  110.9 7.5 %collective-permute-start.9 = (bf16[1,5,1024]{2,1,0:T(8,128)(2,1)S(1)}, bf16[1,5,1024]{2,1,0:T(8,128)(2,1)S(1)}, u32[]{:S(2)}, u32[]{:S(2)}) collective-permute-start(bf16[1,5,1024]{2,1,0:T(8,128)(2,1)S(1)} %get-tuple-element.18), channel_id=1, source_target_pairs={{0,20},{2,22},{4,16},{6,18},{8,28},{10,30},{12,24},{14,26},{16,4},... | collective-permute-start | bytes 30728 | tf_op jit(solution)/shard_map/ppermute | solution.py:202
  111.1 11.1 %collective-permute-start.10 = (bf16[1,5,1024]{2,1,0:T(8,128)(2,1)S(1)}, bf16[1,5,1024]{2,1,0:T(8,128)(2,1)S(1)}, u32[]{:S(2)}, u32[]{:S(2)}) collective-permute-start(bf16[1,5,1024]{2,1,0:T(8,128)(2,1)S(1)} %get-tuple-element.17), channel_id=1, source_target_pairs={{0,22},{2,20},{4,18},{6,16},{8,30},{10,28},{12,26},{14,24},{16,6},... | collective-permute-start | bytes 30728 | tf_op jit(solution)/shard_map/ppermute | solution.py:202
  114.2 8.0 %collective-permute-start.11 = (bf16[1,5,1024]{2,1,0:T(8,128)(2,1)S(1)}, bf16[1,5,1024]{2,1,0:T(8,128)(2,1)S(1)}, u32[]{:S(2)}, u32[]{:S(2)}) collective-permute-start(bf16[1,5,1024]{2,1,0:T(8,128)(2,1)S(1)} %get-tuple-element.16), channel_id=1, source_target_pairs={{0,24},{2,26},{4,28},{6,30},{8,16},{10,18},{12,20},{14,22},{16,8},... | collective-permute-start | bytes 30728 | tf_op jit(solution)/shard_map/ppermute | solution.py:202
  114.2 8.0 %collective-permute-start.12 = (bf16[1,5,1024]{2,1,0:T(8,128)(2,1)S(1)}, bf16[1,5,1024]{2,1,0:T(8,128)(2,1)S(1)}, u32[]{:S(2)}, u32[]{:S(2)}) collective-permute-start(bf16[1,5,1024]{2,1,0:T(8,128)(2,1)S(1)} %get-tuple-element.15), channel_id=1, source_target_pairs={{0,26},{2,24},{4,30},{6,28},{8,18},{10,16},{12,22},{14,20},{16,10}... | collective-permute-start | bytes 30728 | tf_op jit(solution)/shard_map/ppermute | solution.py:202
  118.0 6.5 %collective-permute-start.13 = (bf16[1,5,1024]{2,1,0:T(8,128)(2,1)S(1)}, bf16[1,5,1024]{2,1,0:T(8,128)(2,1)S(1)}, u32[]{:S(2)}, u32[]{:S(2)}) collective-permute-start(bf16[1,5,1024]{2,1,0:T(8,128)(2,1)S(1)} %get-tuple-element.14), channel_id=1, source_target_pairs={{0,28},{2,30},{4,24},{6,26},{8,20},{10,22},{12,16},{14,18},{16,12}... | collective-permute-start | bytes 30728 | tf_op jit(solution)/shard_map/ppermute | solution.py:202
  118.4 6.1 %collective-permute-start.14 = (bf16[1,5,1024]{2,1,0:T(8,128)(2,1)S(1)}, bf16[1,5,1024]{2,1,0:T(8,128)(2,1)S(1)}, u32[]{:S(2)}, u32[]{:S(2)}) collective-permute-start(bf16[1,5,1024]{2,1,0:T(8,128)(2,1)S(1)} %get-tuple-element.13), channel_id=1, source_target_pairs={{0,30},{2,28},{4,26},{6,24},{8,22},{10,20},{12,18},{14,16},{16,14}... | collective-permute-start | bytes 30728 | tf_op jit(solution)/shard_map/ppermute | solution.py:202
Sparse Core Ops, SparseCore 0:
  98.4 87.5 all-reduce.3
